TPU v7x, 32 devices: a whole 2x2x4 slice. The times are simulated.
32 devices in a mesh: grp: 2 (over y), ep: 16 (over z, x, core), tp: 1.
Axes of the slice: x: 2, y: 2, z: 4, core: 2. Of those that a mesh axis runs over, the one named last changes fastest.
Arguments:
- tokens: bfloat16 [2048, 2048], P(('grp', 'ep')), parts along dimension 0, may hold values from -6 to 6
- norm_gain: float32 [2048], replicated, may hold values from 0.1 to 1.9
- routes: int32 [2048, 6], P(('grp', 'ep')), parts along dimension 0, may hold values from 0 to 15, all different within a row; in each aligned block of 64 rows (0 to 63, 64 to 127, ...) at most 48 rows name the same one
- gates: float32 [2048, 6], P(('grp', 'ep')), parts along dimension 0, may hold values from 0.2 to 1
- expert_gate: bfloat16 [16, 2048, 512], P('ep', None, 'tp'), may hold values from -0.125 to 0.125
- expert_up: bfloat16 [16, 2048, 512], P('ep', None, 'tp'), may hold values from -0.125 to 0.125
- expert_down: bfloat16 [16, 512, 2048], P('ep', 'tp'), may hold values from -0.25 to 0.25
- shared_gate: bfloat16 [2048, 512], P(None, 'tp'), may hold values from -0.125 to 0.125
- shared_up: bfloat16 [2048, 512], P(None, 'tp'), may hold values from -0.125 to 0.125
- shared_down: bfloat16 [512, 2048], P('tp'), may hold values from -0.25 to 0.25
Outputs:
- mixed: bfloat16 [2048, 2048], P(('grp', 'ep'), 'tp'), parts along dimension 0
There are 2 independent parts, one for each index of `grp`. A program takes and returns all parts, laid end to end along the dimension named above; an argument that names none is the same for every part. Nothing has to cross between parts.
Inputs may be any that keep to these rules, and one draw needn't show every extreme that they name: `routes`: each row names 6 different experts. In the rows of one index of ep no expert is named by more than 48 rows, and in some such block an expert is named by exactly 48 rows.
All inputs are finite; a program needn't handle non-finite values.
Results may differ from a plain program's by a relative error of at most 0.01.
Values may be sent and summed in bfloat16 or wider, within the bound.
A program may use at most 64 MiB of HBM per device.

v0:
```python
import jax
import jax.numpy as jnp
from jax import lax
from jax.sharding import PartitionSpec as P


def expert_rows(rows, w_gate, w_up, w_down):
    hidden = (
        jax.nn.silu(jnp.einsum("...d,df->...f", rows, w_gate, preferred_element_type=jnp.float32))
        * jnp.einsum("...d,df->...f", rows, w_up, preferred_element_type=jnp.float32)
    ).astype(jnp.bfloat16)
    return jnp.einsum("...f,fd->...d", hidden, w_down, preferred_element_type=jnp.float32).astype(
        jnp.bfloat16
    )


def run_experts(received, ranks, local_experts, expert_gate, expert_up, expert_down):
    count = received.shape[1]
    cols = received.shape[2]
    grouped = received.reshape(ranks, local_experts, count, cols)
    results = jnp.stack(
        [expert_rows(grouped[:, 0], expert_gate[0], expert_up[0], expert_down[0])], axis=1
    )
    return results.reshape(ranks * local_experts, count, results.shape[-1])


def shards(
    tokens,
    norm_gain,
    routes,
    gates,
    expert_gate,
    expert_up,
    expert_down,
    shared_gate,
    shared_up,
    shared_down,
):
    rows_here = tokens.shape[0]
    picks = routes.shape[1]
    local_experts = expert_gate.shape[0]
    ranks = lax.axis_size("ep")
    all_experts = local_experts * ranks
    capacity = max(2, min(rows_here, 2 * rows_here * picks // all_experts))
    values = tokens.astype(jnp.float32)
    scale = lax.rsqrt(jnp.mean(values * values, axis=1, keepdims=True) + 1e-06)
    normed = (values * scale * norm_gain[None, :]).astype(jnp.bfloat16)
    shared_hidden = (
        jax.nn.silu(jnp.dot(normed, shared_gate, preferred_element_type=jnp.float32))
        * jnp.dot(normed, shared_up, preferred_element_type=jnp.float32)
    ).astype(jnp.bfloat16)
    shared_out = jnp.dot(shared_hidden, shared_down, preferred_element_type=jnp.float32)
    flat = routes.reshape(-1)
    matches = (flat[:, None] == jnp.arange(all_experts, dtype=jnp.int32)[None, :]).astype(jnp.int32)
    earlier = jnp.cumsum(matches, axis=0) - matches
    slots = jnp.sum(earlier * matches, axis=1)
    target = flat * capacity + slots
    picker = target[None, :] == jnp.arange(all_experts * capacity, dtype=jnp.int32)[:, None]
    picker = picker.reshape(all_experts * capacity, rows_here, picks)
    take_rows = jnp.any(picker, axis=2).astype(jnp.bfloat16)
    buffer = jnp.dot(take_rows, normed, preferred_element_type=jnp.float32).astype(jnp.bfloat16)
    buffer = buffer.reshape(all_experts, capacity, normed.shape[1])
    results = run_experts(
        lax.all_to_all(buffer, "ep", split_axis=0, concat_axis=0, tiled=True),
        ranks,
        local_experts,
        expert_gate,
        expert_up,
        expert_down,
    )
    returned = lax.all_to_all(results, "ep", split_axis=0, concat_axis=0, tiled=True)
    flat_back = returned.reshape(all_experts * capacity, returned.shape[2])
    picked = flat_back[target].reshape(rows_here, picks, returned.shape[2]).astype(jnp.float32)
    routed = jnp.sum(gates[:, :, None] * picked, axis=1)
    payload = routed + shared_out
    summed = lax.psum_scatter(payload.astype(jnp.bfloat16), "tp", scatter_dimension=1, tiled=True)
    return summed


def solution(mesh):
    in_specs = (
        P(("grp", "ep"), None),
        P(),
        P(("grp", "ep"), None),
        P(("grp", "ep"), None),
        P("ep", None, "tp"),
        P("ep", None, "tp"),
        P("ep", "tp", None),
        P(None, "tp"),
        P(None, "tp"),
        P("tp", None),
    )
    out_specs = P(("grp", "ep"), "tp")
    return jax.shard_map(shards, mesh=mesh, in_specs=in_specs, out_specs=out_specs, check_vma=False)
```

profile of v0, /device:TPU:11, one launch (start us, length us, event | category | flops | bytes accessed | tf_op | source)
XLA Modules:
  0.0 189.2 jit_solution(11217187855555702786)
XLA Ops:
  0.0 0.0 copy-start
  0.0 0.9 copy.19
  0.9 0.1 eq.43
  1.1 0.1 eq.39
  1.2 0.9 reduce-window.6
  2.1 0.2 slice_reduce_fusion
  2.3 0.1 fusion.23
  2.4 0.1 reduce_sum.32
  2.6 0.1 copy.23
  2.7 0.2 fusion.8
  2.9 1.1 fusion.12
  4.1 2.0 %convolution_convert_fusion.1 = bf16[768,2048]{1,0:T(8,128)(2,1)S(1)} fusion(pred[768,64]{0,1:T(8,128)(4,1)S(1)} %fusion.8, bf16[64,2048]{1,0:T(8,128)(2,1)} %param.10, f32[2048]{0:T(1024)} %param.11, f32[64]{0:T(128)S(1)} %add_rsqrt_fusion), kind=kOutput, calls=%fused_computation.3 | convolution fusion | flops 203423744 | bytes 3465472 | tf_op jit(solution)/shard_map/dot_general | solution.py:61
  6.1 0.0 copy-start.5
  6.1 76.2 %all_to_all.10 = bf16[16,48,2048]{2,1,0:T(8,128)(2,1)S(1)} all-to-all(bf16[16,48,2048]{2,1,0:T(8,128)(2,1)S(1)} %bitcast.44), channel_id=1, replica_groups=mesh['grp'=2,'ep'=16,'tp'=1] {'ep'}, dimensions={0} | all-to-all | bytes 6291456 | tf_op jit(solution)/shard_map/all_to_all | solution.py:64
  82.3 0.0 copy-start.2
  82.3 1.7 copy-done.2
  84.0 0.0 copy-done.5
  84.0 2.9 %fusion.4 = f32[16,48,512]{2,1,0:T(8,128)} fusion(bf16[16,48,2048]{2,1,0:T(8,128)(2,1)S(1)} %all_to_all.10, bf16[1,2048,512]{2,1,0:T(8,128)(2,1)S(1)} %copy-done.5), kind=kOutput, calls=%fused_computation.9 | convolution fusion | flops 1610612736 | bytes 6815744 | tf_op jit(solution)/shard_map/...d,df->...f/dot_general | solution.py:9
  86.9 0.0 copy-done
  86.9 8.1 %convolution_convert_fusion = bf16[16,48,2048]{2,1,0:T(8,128)(2,1)} fusion(bf16[1,512,2048]{2,1,0:T(8,128)(2,1)S(1)} %copy-done, f32[16,48,512]{2,1,0:T(8,128)} %fusion.4, bf16[16,48,2048]{2,1,0:T(8,128)(2,1)} %copy-done.2, bf16[1,2048,512]{2,1,0:T(8,128)(2,1)} %param.15), kind=kOutput, calls=%fused_computation.2 | convolution fusion | flops 3225157632 | bytes 12058624 | tf_op jit(solution)/shard_map/...f,fd->...d/dot_general | solution.py:12
  95.0 0.0 copy-start.4
  95.1 0.0 copy-start.1
  95.1 0.0 copy-start.3
  95.1 5.2 %all-to-all-start.1 = ((bf16[16,48,2048]{2,1,0:T(8,128)(2,1)}), bf16[16,48,2048]{2,1,0:T(8,128)(2,1)}, u32[]{:S(2)}, u32[]{:S(2)}) async-start(bf16[16,48,2048]{2,1,0:T(8,128)(2,1)} %convolution_convert_fusion), calls=%async_computation.1 | async-start | bytes 6291456 | tf_op jit(solution)/shard_map/all_to_all | solution.py:71
  100.3 0.1 mul.75
  100.4 0.0 copy-done.4
  100.4 0.1 copy.18
  100.6 0.0 copy-done.1
  100.6 0.0 copy-done.3
  100.6 2.1 %fusion.31 = f32[64,512]{1,0:T(8,128)S(1)} fusion(bf16[2048,512]{1,0:T(8,128)(2,1)} %param.17, bf16[64,2048]{1,0:T(8,128)(2,1)S(1)} %copy-done.1, f32[2048]{0:T(1024)S(1)} %copy-done.3, f32[64]{0:T(128)S(1)} %add_rsqrt_fusion), kind=kOutput, calls=%fused_computation.44 | convolution fusion | flops 134742016 | bytes 2498816 | tf_op jit(solution)/shard_map/dot_general | solution.py:49
  102.7 67.6 %all-to-all-done.1 = bf16[16,48,2048]{2,1,0:T(8,128)(2,1)} async-done(((bf16[16,48,2048]{2,1,0:T(8,128)(2,1)}), bf16[16,48,2048]{2,1,0:T(8,128)(2,1)}, u32[]{:S(2)}, u32[]{:S(2)}) %all-to-all-start.1) | async-done | bytes 3145760 | tf_op jit(solution)/shard_map/all_to_all | solution.py:71
  170.3 7.3 %gather_fusion = bf16[384,2048]{1,0:T(8,128)(2,1)} fusion(bf16[768,2048]{1,0:T(8,128)(2,1)} %bitcast.8, s32[1024]{0:T(1024)S(1)} %pad_clamp_fusion), kind=kCustom, calls=%fused_computation | custom fusion | bytes 3147264 | tf_op jit(solution)/shard_map/gather | solution.py:73
  177.6 3.9 %reshape.85 = f32[64,6,2048]{2,1,0:T(8,128)} reshape(bf16[384,2048]{1,0:T(8,128)(2,1)} %gather_fusion) | data formatting | bytes 4718592 | tf_op jit(solution)/shard_map/convert_element_type | solution.py:73
  181.5 3.7 %multiply_reduce_fusion = f32[64,2048]{1,0:T(8,128)S(1)} fusion(f32[64,6,2048]{2,1,0:T(8,128)} %reshape.85, f32[64,6]{1,0:T(8,128)S(1)} %copy.18), kind=kLoop, calls=%fused_computation.1 | loop fusion | flops 1441792 | bytes 3671552 | tf_op jit(solution)/shard_map/reduce_sum | solution.py:74
  185.3 3.9 %fusion = bf16[64,2048]{1,0:T(8,128)(2,1)} fusion(f32[64,2048]{1,0:T(8,128)S(1)} %multiply_reduce_fusion, bf16[512,2048]{1,0:T(8,128)(2,1)} %param.19, bf16[2048,512]{1,0:T(8,128)(2,1)} %param.18, f32[64,512]{1,0:T(8,128)S(1)} %fusion.31, bf16[64,2048]{1,0:T(8,128)(2,1)S(1)} %copy-done.1, f32[2048]{0:T(1024)S(1)} %copy-done.3, f32[64]{0:T(128)S(1)} %add_rsqrt_fusion), kind=kOutput, calls=%fused_computation.5 | convolution fusion | flops 269418496 | bytes 5382400 | tf_op jit(solution)/shard_map/dot_general | solution.py:52
  (6 shorter events, 0.1 us)
Async XLA Ops:
  0.0 86.9 %copy-start = (bf16[1,512,2048]{2,1,0:T(8,128)(2,1)S(1)}, bf16[1,512,2048]{2,1,0:T(8,128)(2,1)}, u32[]{:S(2)}) copy-start(bf16[1,512,2048]{2,1,0:T(8,128)(2,1)} %param.16) | copy-start | bytes 6291460
  6.1 77.9 %copy-start.5 = (bf16[1,2048,512]{2,1,0:T(8,128)(2,1)S(1)}, bf16[1,2048,512]{2,1,0:T(8,128)(2,1)}, u32[]{:S(2)}) copy-start(bf16[1,2048,512]{2,1,0:T(8,128)(2,1)} %param.14) | copy-start | bytes 6291460
  82.3 1.7 copy-start.2
  95.0 5.4 %copy-start.4 = (f32[64,6]{0,1:T(8,128)S(1)}, f32[64,6]{0,1:T(8,128)}, u32[]{:S(2)}) copy-start(f32[64,6]{0,1:T(8,128)} %param.13) | copy-start | bytes 4612
  95.1 5.5 %copy-start.1 = (bf16[64,2048]{1,0:T(8,128)(2,1)S(1)}, bf16[64,2048]{1,0:T(8,128)(2,1)}, u32[]{:S(2)}) copy-start(bf16[64,2048]{1,0:T(8,128)(2,1)} %param.10) | copy-start | bytes 786436
  95.1 5.5 %copy-start.3 = (f32[2048]{0:T(1024)S(1)}, f32[2048]{0:T(1024)}, u32[]{:S(2)}) copy-start(f32[2048]{0:T(1024)} %param.11) | copy-start | bytes 24580
  95.1 75.2 %all-to-all-start.1 = ((bf16[16,48,2048]{2,1,0:T(8,128)(2,1)}), bf16[16,48,2048]{2,1,0:T(8,128)(2,1)}, u32[]{:S(2)}, u32[]{:S(2)}) async-start(bf16[16,48,2048]{2,1,0:T(8,128)(2,1)} %convolution_convert_fusion), calls=%async_computation.1 | async-start | bytes 6291456 | tf_op jit(solution)/shard_map/all_to_all | solution.py:71
where the time goes:
time: 190 us; the launch traced here: 189 us
  blocking collectives  76.2 us (40%)
  waiting for transfers between devices  67.6 us (36%)
  matrix products  19.1 us (10%)
  local copies, waits for them, and re-layouts  14.8 us (8%)
  other arithmetic  6.15 us (3%)
  starting transfers between devices  5.24 us (3%)
    all_to_all x1, blocking collectives, shards(): lax.all_to_all(buffer, 'ep', split_axis=0, concat_axis=0, tiled=True)  76.2 us
    all_to_all x1, waiting for transfers between devices, shards(): lax.all_to_all(results, 'ep', split_axis=0, concat_axis=0, tiled=True)  67.6 us
    dot_general x1, matrix products, expert_rows(): jnp.einsum('...f,fd->...d', hidden, w_down, preferred_element_type=jnp.fl...  8.14 us
    gather x1, local copies, waits for them, and re-layouts, shards(): flat_back[target].reshape(rows_here, picks, returned.shape[2])  7.34 us
    all_to_all x1, starting transfers between devices, shards(): lax.all_to_all(results, 'ep', split_axis=0, concat_axis=0, tiled=True)  5.24 us
    convert_element_type x1, local copies, waits for them, and re-layouts, shards(): flat_back[target].reshape(rows_here, picks, returned.shape[2])  3.89 us
    dot_general x1, matrix products, shards(): jnp.dot(shared_hidden, shared_down, preferred_element_type=jnp.float32)  3.89 us
  transfers between devices with their start and end apart: 1, of which 1 were waited for; matrix products, arithmetic and copies ran while one was open for 1% of the time, Pallas kernels for 0%

commit v1 on v0

--- a/solution.py
+++ b/solution.py
@@ -77,6 +77,53 @@
     return summed
 
 
+def dense_shards(
+    tokens,
+    norm_gain,
+    routes,
+    gates,
+    expert_gate,
+    expert_up,
+    expert_down,
+    shared_gate,
+    shared_up,
+    shared_down,
+):
+    cols = tokens.shape[1]
+    experts = lax.axis_size("ep")
+    me = lax.axis_index("ep")
+    values = tokens.astype(jnp.float32)
+    scale = lax.rsqrt(jnp.mean(values * values, axis=1, keepdims=True) + 1e-06)
+    normed = (values * scale * norm_gain[None, :]).astype(jnp.bfloat16)
+    lanes = jnp.arange(experts, dtype=jnp.int32)
+    weight = jnp.sum(
+        jnp.where(routes[:, :, None] == lanes[None, None, :], gates[:, :, None], 0.0), axis=1
+    )
+    high = weight.astype(jnp.bfloat16)
+    low = (weight - high.astype(jnp.float32)).astype(jnp.bfloat16)
+    gathered = lax.all_gather(
+        jnp.concatenate([normed, high, low], axis=1), "ep", axis=0, tiled=True
+    )
+    tail = gathered[:, cols:].astype(jnp.float32)
+    places = jnp.arange(2 * experts, dtype=jnp.int32)
+    mine = jnp.sum(jnp.where((places % experts == me)[None, :], tail, 0.0), axis=1, keepdims=True)
+    rows = gathered[:, :cols]
+    hidden = (
+        jax.nn.silu(jnp.dot(rows, expert_gate[0], preferred_element_type=jnp.float32))
+        * jnp.dot(rows, expert_up[0], preferred_element_type=jnp.float32)
+    ).astype(jnp.bfloat16)
+    partial = jnp.dot(hidden, expert_down[0], preferred_element_type=jnp.float32)
+    shared_hidden = (
+        jax.nn.silu(jnp.dot(normed, shared_gate, preferred_element_type=jnp.float32))
+        * jnp.dot(normed, shared_up, preferred_element_type=jnp.float32)
+    ).astype(jnp.bfloat16)
+    shared_out = jnp.dot(shared_hidden, shared_down, preferred_element_type=jnp.float32)
+    routed = lax.psum_scatter(
+        (partial * mine).astype(jnp.bfloat16), "ep", scatter_dimension=0, tiled=True
+    )
+    return (routed.astype(jnp.float32) + shared_out).astype(jnp.bfloat16)
+
+
 def solution(mesh):
     in_specs = (
         P(("grp", "ep"), None),
@@ -91,4 +138,5 @@
         P("tp", None),
     )
     out_specs = P(("grp", "ep"), "tp")
-    return jax.shard_map(shards, mesh=mesh, in_specs=in_specs, out_specs=out_specs, check_vma=False)
+    body = dense_shards if mesh.shape['tp'] == 1 else shards
+    return jax.shard_map(body, mesh=mesh, in_specs=in_specs, out_specs=out_specs, check_vma=False)

time: 190 us -> 165 us (0.87)
  the two profiles are of different devices: /device:TPU:11 before, /device:TPU:0 now
where the time goes in v1:
time: 165 us
  waiting for transfers between devices  124 us (75%)
  matrix products  22.5 us (14%)
  between operations  13.5 us (8%)
  other arithmetic  4.18 us (3%)
    reduce_scatter x1, waiting for transfers between devices, dense_shards(): lax.psum_scatter((partial * mine).astype(jnp.bfloat16), 'ep', scatter_dim...  69.4 us
    all_gather x1, waiting for transfers between devices, dense_shards(): lax.all_gather(jnp.concatenate([normed, high, low], axis=1), 'ep', axis=0...  54.5 us
    dot_general x1, matrix products, dense_shards(): jnp.dot(hidden, expert_down[0], preferred_element_type=jnp.float32)  10 us
    dot_general x1, matrix products, dense_shards(): jnp.dot(rows, expert_gate[0], preferred_element_type=jnp.float32)  6.56 us
    dot_general x1, matrix products, dense_shards(): jnp.dot(shared_hidden, shared_down, preferred_element_type=jnp.float32)  3.84 us
  transfers between devices with their start and end apart: 2, of which 2 were waited for; matrix products, arithmetic and copies ran while one was open for 1% of the time, Pallas kernels for 0%

profile of v1, /device:TPU:0, one launch (start us, length us, event | category | flops | bytes accessed | tf_op | source)
XLA Modules:
  0.0 165.1 jit_solution(11798139883453189109)
XLA Ops:
  6.5 0.0 copy-start
  6.5 0.0 all-gather.2.cloned.1.call-start
  6.5 1.2 fusion.17
  7.8 0.7 select_reduce_fusion.1
  8.5 0.1 copy.13
  8.6 0.1 copy.14
  8.7 1.1 fusion.19
  9.8 0.8 concatenate.3
  10.6 0.0 all-gather.2.cloned.1.call-update
  10.7 0.0 reduce-scatter.2.cloned.1.call-start
  10.7 54.5 %all-gather.2.cloned.1.call-done = bf16[1024,2080]{1,0:T(8,128)(2,1)} async-done(((bf16[64,2080]{1,0:T(8,128)(2,1)}), bf16[1024,2080]{1,0:T(8,128)(2,1)}) %all-gather.2.cloned.1.call-update) | async-done | bytes 4259856 | tf_op jit(solution)/shard_map/all_gather | solution.py:104
  65.2 6.6 %fusion.2 = f32[1024,512]{1,0:T(8,128)} fusion(bf16[1024,2080]{1,0:T(8,128)(2,1)} %all-gather.2.cloned.1.call-done, bf16[1,2048,512]{2,1,0:T(8,128)(2,1)} %param.14), kind=kOutput, calls=%fused_computation.3 | convolution fusion | flops 2147483648 | bytes 8388608 | tf_op jit(solution)/shard_map/dot_general | solution.py:112
  71.8 1.1 select_reduce_fusion
  72.9 0.0 copy-done
  72.9 10.0 %multiply_convert_fusion = bf16[1024,2048]{1,0:T(8,128)(2,1)} fusion(f32[1024]{0:T(1024)S(1)} %select_reduce_fusion, bf16[1,512,2048]{2,1,0:T(8,128)(2,1)S(1)} %copy-done, f32[1024,512]{1,0:T(8,128)} %fusion.2, bf16[1,2048,512]{2,1,0:T(8,128)(2,1)} %param.15, bf16[1024,2080]{1,0:T(8,128)(2,1)} %all-gather.2.cloned.1.call-done), kind=kOutput, calls=%fused_computation | convolution fusion | flops 4302307328 | bytes 14684160 | tf_op jit(solution)/shard_map/dot_general | solution.py:115
  82.9 0.0 reduce-scatter.2.cloned.1.call-update
  82.9 2.1 %fusion.29 = f32[64,512]{1,0:T(8,128)S(1)} fusion(bf16[64,2048]{1,0:T(8,128)(2,1)S(1)} %fusion.19, bf16[2048,512]{1,0:T(8,128)(2,1)} %param.17), kind=kOutput, calls=%fused_computation.33 | convolution fusion | flops 134217728 | bytes 2490368 | tf_op jit(solution)/shard_map/dot_general | solution.py:117
  85.0 69.4 %reduce-scatter.2.cloned.1.call-done = bf16[64,2048]{1,0:T(8,128)(2,1)} async-done(((bf16[1024,2048]{1,0:T(8,128)(2,1)}), bf16[64,2048]{1,0:T(8,128)(2,1)}) %reduce-scatter.2.cloned.1.call-update) | async-done | bytes 262160 | tf_op jit(solution)/shard_map/reduce_scatter | solution.py:121
  154.4 3.8 %fusion.4 = bf16[64,2048]{1,0:T(8,128)(2,1)} fusion(bf16[512,2048]{1,0:T(8,128)(2,1)} %param.19, bf16[64,2048]{1,0:T(8,128)(2,1)S(1)} %fusion.19, bf16[2048,512]{1,0:T(8,128)(2,1)} %param.18, bf16[64,2048]{1,0:T(8,128)(2,1)} %reduce-scatter.2.cloned.1.call-done, f32[64,512]{1,0:T(8,128)S(1)} %fusion.29), kind=kOutput, calls=%fused_computation.6 | convolution fusion | flops 269025280 | bytes 5111808 | tf_op jit(solution)/shard_map/dot_general | solution.py:120
  (3 shorter events, 0.0 us)
Async XLA Ops:
  6.5 66.3 %copy-start = (bf16[1,512,2048]{2,1,0:T(8,128)(2,1)S(1)}, bf16[1,512,2048]{2,1,0:T(8,128)(2,1)}, u32[]{:S(2)}) copy-start(bf16[1,512,2048]{2,1,0:T(8,128)(2,1)} %param.16) | copy-start | bytes 6291460
  6.5 58.7 %all-gather.2.cloned.1.call-start = ((), (), s32[]{:S(2)}) async-start(), calls=%async_computation.1 | async-start | bytes 4734976 | tf_op jit(solution)/shard_map/all_gather | solution.py:104
  10.7 143.8 %reduce-scatter.2.cloned.1.call-start = ((), (), s32[]{:S(2)}) async-start(), calls=%async_computation.2 | async-start | bytes 4456448 | tf_op jit(solution)/shard_map/reduce_scatter | solution.py:121
Sparse Core Ops, SparseCore 0:
  10.8 54.3 all-gather.1
  83.0 71.3 reduce-scatter.1

commit v2 on v0

--- a/solution.py
+++ b/solution.py
@@ -1,6 +1,10 @@
+import functools
+
 import jax
 import jax.numpy as jnp
 from jax import lax
+from jax.experimental import pallas as pl
+from jax.experimental.pallas import tpu as pltpu
 from jax.sharding import PartitionSpec as P
 
 
@@ -77,6 +81,449 @@
     return summed
 
 
+def fused_kernel(
+    nz,
+    pieces,
+    tokens,
+    gain,
+    routes,
+    gates,
+    eg_hbm,
+    eu_hbm,
+    ed_hbm,
+    sg_hbm,
+    su_hbm,
+    sd_hbm,
+    out,
+    ag,
+    eg,
+    eu,
+    ed,
+    sg,
+    su,
+    sd,
+    shared,
+    keep,
+    psend,
+    rs_d,
+    sx,
+    rs_x,
+    sz,
+    chain,
+    wsem,
+    z_send,
+    z_recv,
+    x_send,
+    x_recv,
+    d_send,
+    d_recv,
+    rd_send,
+    rd_recv,
+    rx_send,
+    rx_recv,
+    rz_send,
+    rz_recv,
+):
+    rows, cols = tokens.shape
+    experts = 4 * nz
+    me = lax.axis_index("ep")
+    z, x, c = me // 4, (me // 2) % 2, me % 2
+    partner = 4 * z + 2 * x + (1 - c)
+    across = 4 * z + 2 * (1 - x) + c
+    up, down = jnp.minimum(z + 1, nz - 1) * 4 + 2 * x + c, jnp.maximum(z - 1, 0) * 4 + 2 * x + c
+
+    loads = [
+        pltpu.make_async_copy(src, dst, wsem.at[i])
+        for i, (src, dst) in enumerate(
+            [(sg_hbm, sg), (su_hbm, su), (sd_hbm, sd), (eg_hbm, eg), (eu_hbm, eu), (ed_hbm, ed)]
+        )
+    ]
+    for load in loads:
+        load.start()
+
+    def remote(src, dst, send, recv, to):
+        return pltpu.make_async_remote_copy(
+            src_ref=src,
+            dst_ref=dst,
+            send_sem=send,
+            recv_sem=recv,
+            device_id={"ep": to},
+            device_id_type=pl.DeviceIdType.MESH,
+        )
+
+    def part(p, rc, rx):
+        start, size, _ = pieces[p]
+        return pl.ds((rc * 2 + rx) * rows + start, size)
+
+    def ag_z(layer, rx, p, way):
+        ref = ag.at[layer, part(p, 0, rx)]
+        to = up if way == 0 else down
+        return remote(ref, ref, z_send.at[way, layer, rx, p], z_recv.at[layer, rx, p], to)
+
+    def ag_x(layer, p):
+        return remote(
+            ag.at[layer, part(p, 0, 0)],
+            ag.at[layer, part(p, 0, 1)],
+            x_send.at[layer, p],
+            x_recv.at[layer, p],
+            across,
+        )
+
+    def ag_d(layer, rx, p):
+        return remote(
+            ag.at[layer, part(p, 0, rx)],
+            ag.at[layer, part(p, 1, rx)],
+            d_send.at[layer, rx, p],
+            d_recv.at[layer, rx, p],
+            partner,
+        )
+
+    def rs_core(layer):
+        return remote(
+            psend.at[layer], rs_d.at[layer], rd_send.at[layer], rd_recv.at[layer], partner
+        )
+
+    def rs_across(layer, p):
+        ds = part(p, 0, 0)
+        return remote(
+            sx.at[layer, ds], rs_x.at[layer, ds], rx_send.at[layer, p], rx_recv.at[layer, p], across
+        )
+
+    def rs_z(layer, rx, p, way):
+        ds = part(p, 0, rx)
+        to = up if way == 0 else down
+        return remote(
+            sz.at[layer, ds],
+            chain.at[way, layer, ds],
+            rz_send.at[layer, rx, p],
+            rz_recv.at[way, layer, rx, p],
+            to,
+        )
+
+    count = range(len(pieces))
+    kinds = [(p, rx) for p in count for rx in ((0, 1) if pieces[p][2] else (0,))]
+
+    def has(way):
+        return z < nz - 1 if way == 0 else z > 0
+
+    barrier = pltpu.get_barrier_semaphore()
+    for to in (partner, across):
+        pl.semaphore_signal(
+            barrier, inc=1, device_id={"ep": to}, device_id_type=pl.DeviceIdType.MESH
+        )
+    for way, to in ((0, up), (1, down)):
+
+        @pl.when(has(way))
+        def _():
+            pl.semaphore_signal(
+                barrier, inc=1, device_id={"ep": to}, device_id_type=pl.DeviceIdType.MESH
+            )
+
+    values = tokens[...].astype(jnp.float32)
+    scale = lax.rsqrt(jnp.mean(values * values, axis=1, keepdims=True) + 1e-06)
+    normed = (values * scale * gain[...]).astype(jnp.bfloat16)
+    width = ag.shape[2] - cols
+    lane = lax.broadcasted_iota(jnp.int32, (rows, width), 1)
+    expert = lane % experts
+    weight = jnp.zeros((rows, width), jnp.float32)
+    for k in range(routes.shape[1]):
+        weight += jnp.where(expert == routes[:, k : k + 1], gates[:, k : k + 1], 0.0)
+    high = weight.astype(jnp.bfloat16).astype(jnp.float32)
+    tail = jnp.where(lane < experts, high, jnp.where(lane < 2 * experts, weight - high, 0.0))
+    ag[z, :rows, :cols] = normed
+    ag[z, :rows, cols:] = tail.astype(jnp.bfloat16)
+
+    peers = 2 + jnp.minimum(z, 1) + jnp.minimum(nz - 1 - z, 1)
+    pl.semaphore_wait(barrier, peers)
+
+    for p in sorted(count, key=lambda p: not pieces[p][2]):
+        ag_x(z, p).start()
+        for way in (0, 1):
+
+            @pl.when(has(way))
+            def _():
+                ag_z(z, 0, p, way).start()
+
+        ag_d(z, 0, p).start()
+
+    for load in loads[:3]:
+        load.wait()
+    mine = ag[z, :rows, :cols]
+    gate = jnp.dot(mine, sg[...], preferred_element_type=jnp.float32)
+    lift = jnp.dot(mine, su[...], preferred_element_type=jnp.float32)
+    hidden = (jax.nn.silu(gate) * lift).astype(jnp.bfloat16)
+    shared[...] = jnp.dot(hidden, sd[...], preferred_element_type=jnp.float32)
+
+    for p in sorted(count, key=lambda p: not pieces[p][2]):
+        ag_x(z, p).wait_recv()
+        ag_d(z, 1, p).start()
+        if pieces[p][2]:
+            for way in (0, 1):
+
+                @pl.when(has(way))
+                def _():
+                    ag_z(z, 1, p, way).start()
+
+    for load in loads[3:]:
+        load.wait()
+
+    def at_distance(d, body):
+        for way, layer, inside in ((0, z - d, z - d >= 0), (1, z + d, z + d < nz)):
+
+            @pl.when(inside)
+            def _():
+                body(layer, way)
+
+    def forward(layer, way):
+        for p, rx in kinds:
+            ag_z(layer, rx, p, way).wait_recv()
+
+            @pl.when(has(way))
+            def _():
+                ag_z(layer, rx, p, way).start()
+
+            if not pieces[p][2]:
+                ag_x(layer, p).start()
+            ag_d(layer, rx, p).start()
+
+    def relay(layer, way):
+        for p in count:
+            if not pieces[p][2]:
+                ag_x(layer, p).wait_recv()
+                ag_d(layer, 1, p).start()
+
+    def pick(table, k):
+        found = 0
+        for i, line in enumerate(table):
+            for j, layer in enumerate(line):
+                found = jnp.where(jnp.logical_and(z == i, k == j), layer, found)
+        return found
+
+    inner = [
+        list(range(i + 1, nz)) + list(range(i - 1, -1, -1))
+        if 2 * i < nz
+        else list(range(i - 1, -1, -1)) + list(range(i + 1, nz))
+        for i in range(nz)
+    ]
+    order = [
+        [i] + sorted(inner[i], key=lambda layer: abs(layer - i)) for i in range(nz)
+    ]
+
+    def experts_on(layer):
+        for p in count:
+            for rx in (0, 1):
+                ag_d(layer, rx, p).wait_recv()
+        block = ag[layer, :, :cols]
+        tails = ag[layer, :, cols:].astype(jnp.float32)
+        spot = lax.broadcasted_iota(jnp.int32, tails.shape, 1) % experts
+        share = jnp.sum(jnp.where(spot == me, tails, 0.0), axis=1, keepdims=True)
+        a = jnp.dot(block, eg[...], preferred_element_type=jnp.float32)
+        b = jnp.dot(block, eu[...], preferred_element_type=jnp.float32)
+        h = (jax.nn.silu(a) * b).astype(jnp.bfloat16)
+        step = cols // 4
+        for i in range(4):
+            cs = slice(i * step, (i + 1) * step)
+            y = jnp.dot(h, ed[:, cs], preferred_element_type=jnp.float32) * share
+            keep[layer, :, cs] = y[: 2 * rows]
+            psend[layer, :, cs] = y[2 * rows :].astype(jnp.bfloat16)
+        rs_core(layer).start()
+
+    def fold_core(layer):
+        rs_core(layer).wait_recv()
+        for p in count:
+            if not pieces[p][2]:
+                ds = part(p, 0, 1)
+                both = keep[layer, ds] + rs_d[layer, ds].astype(jnp.float32)
+                sx[layer, part(p, 0, 0)] = both.astype(jnp.bfloat16)
+                rs_across(layer, p).start()
+
+    def local_sum(layer, rx, p):
+        ds = part(p, 0, rx)
+        total = keep[layer, ds] + rs_d[layer, ds].astype(jnp.float32)
+        if not pieces[p][2]:
+            total += rs_x[layer, ds].astype(jnp.float32)
+        return total
+
+    def send_sum(layer):
+        for way in (0, 1):
+            arrives = z > 0 if way == 0 else z < nz - 1
+
+            @pl.when(layer > z if way == 0 else layer < z)
+            def _():
+                for p, rx in kinds:
+                    ds = part(p, 0, rx)
+                    if not pieces[p][2]:
+                        rs_across(layer, p).wait_recv()
+
+                    @pl.when(arrives)
+                    def _():
+                        rs_z(layer, rx, p, way).wait_recv()
+                        more = chain[way, layer, ds].astype(jnp.float32)
+                        sz[layer, ds] = (local_sum(layer, rx, p) + more).astype(jnp.bfloat16)
+
+                    @pl.when(jnp.logical_not(arrives))
+                    def _():
+                        sz[layer, ds] = local_sum(layer, rx, p).astype(jnp.bfloat16)
+
+                    rs_z(layer, rx, p, way).start()
+
+    edge = jnp.logical_or(z == 0, z == nz - 1)
+
+    @pl.loop(0, nz)
+    def _(k):
+        at_distance(k + 1, forward)
+        experts_on(pick(order, k))
+        at_distance(k + 1, relay)
+
+        @pl.when(k >= 1)
+        def _():
+            fold_core(pick(order, k - 1))
+
+        @pl.when(jnp.logical_and(k >= 2, edge))
+        def _():
+            send_sum(pick(order, k - 1))
+
+    fold_core(pick(order, nz - 1))
+
+    @pl.loop(0, nz - 1)
+    def _(j):
+        @pl.when(jnp.logical_or(jnp.logical_not(edge), j == nz - 2))
+        def _():
+            send_sum(pick(inner, j))
+
+    def add_chains(p, rx):
+        ds = part(p, 0, rx)
+        for way in (0, 1):
+
+            @pl.when(z > 0 if way == 0 else z < nz - 1)
+            def _():
+                rs_z(z, rx, p, way).wait_recv()
+                keep[z, ds] = keep[z, ds] + chain[way, z, ds].astype(jnp.float32)
+
+    for p in count:
+        if pieces[p][2]:
+            add_chains(p, 1)
+            sx[z, part(p, 0, 0)] = local_sum(z, 1, p).astype(jnp.bfloat16)
+            rs_across(z, p).start()
+    for p in sorted(count, key=lambda p: pieces[p][2]):
+        ds = part(p, 0, 0)
+        add_chains(p, 0)
+        rs_across(z, p).wait_recv()
+        total = local_sum(z, 0, p) + shared[ds]
+        if pieces[p][2]:
+            total += rs_x[z, ds].astype(jnp.float32)
+        out[ds] = total.astype(out.dtype)
+
+    @pl.loop(0, nz)
+    def _(layer):
+        for p in count:
+            for rx in (0, 1):
+                ag_d(layer, rx, p).wait_send()
+            if not pieces[p][2]:
+                ag_x(layer, p).wait_send()
+                rs_across(layer, p).wait_send()
+            else:
+
+                @pl.when(layer == z)
+                def _():
+                    ag_x(layer, p).wait_send()
+                    rs_across(layer, p).wait_send()
+
+        rs_core(layer).wait_send()
+        for way in (0, 1):
+            behind = layer <= z if way == 0 else layer >= z
+            ahead = layer > z if way == 0 else layer < z
+
+            @pl.when(jnp.logical_and(behind, has(way)))
+            def _():
+                for p, rx in kinds:
+                    ag_z(layer, rx, p, way).wait_send()
+
+            @pl.when(ahead)
+            def _():
+                for p, rx in kinds:
+                    rs_z(layer, rx, p, way).wait_send()
+
+
+def fused_shards(
+    tokens,
+    norm_gain,
+    routes,
+    gates,
+    expert_gate,
+    expert_up,
+    expert_down,
+    shared_gate,
+    shared_up,
+    shared_down,
+):
+    rows, cols = tokens.shape
+    ff = expert_gate.shape[2]
+    shared_ff = shared_gate.shape[1]
+    ranks = lax.axis_size("ep")
+    nz = ranks // 4
+    pieces = make_pieces(rows)
+    count = len(pieces)
+    width = cols + -(-2 * ranks // 128) * 128
+    half, narrow = jnp.bfloat16, pltpu.SemaphoreType.DMA
+    vmem, anywhere = pl.BlockSpec(memory_space=pltpu.VMEM), pl.BlockSpec(memory_space=pl.ANY)
+    return pl.pallas_call(
+        functools.partial(fused_kernel, nz, pieces),
+        out_shape=jax.ShapeDtypeStruct((rows, cols), half),
+        in_specs=[vmem] * 4 + [anywhere] * 6,
+        out_specs=vmem,
+        scratch_shapes=[
+            pltpu.VMEM((nz, 4 * rows, width), half),
+            pltpu.VMEM((cols, ff), half),
+            pltpu.VMEM((cols, ff), half),
+            pltpu.VMEM((ff, cols), half),
+            pltpu.VMEM((cols, shared_ff), half),
+            pltpu.VMEM((cols, shared_ff), half),
+            pltpu.VMEM((shared_ff, cols), half),
+            pltpu.VMEM((rows, cols), jnp.float32),
+            pltpu.VMEM((nz, 2 * rows, cols), jnp.float32),
+            pltpu.VMEM((nz, 2 * rows, cols), half),
+            pltpu.VMEM((nz, 2 * rows, cols), half),
+            pltpu.VMEM((nz, rows, cols), half),
+            pltpu.VMEM((nz, rows, cols), half),
+            pltpu.VMEM((nz, 2 * rows, cols), half),
+            pltpu.VMEM((2, nz, 2 * rows, cols), half),
+            narrow((6,)),
+            narrow((2, nz, 2, count)),
+            narrow((nz, 2, count)),
+            narrow((nz, count)),
+            narrow((nz, count)),
+            narrow((nz, 2, count)),
+            narrow((nz, 2, count)),
+            narrow((nz,)),
+            narrow((nz,)),
+            narrow((nz, count)),
+            narrow((nz, count)),
+            narrow((nz, 2, count)),
+            narrow((2, nz, 2, count)),
+        ],
+        compiler_params=pltpu.CompilerParams(
+            collective_id=0, has_side_effects=True, vmem_limit_bytes=60 * 1024 * 1024
+        ),
+    )(
+        tokens,
+        norm_gain[None, :],
+        routes,
+        gates,
+        expert_gate[0],
+        expert_up[0],
+        expert_down[0],
+        shared_gate,
+        shared_up,
+        shared_down,
+    )
+
+
+def make_pieces(rows):
+    unit = rows // 4
+    return [(0, 2 * unit, False), (2 * unit, unit, False), (3 * unit, unit, True)]
+
+
 def solution(mesh):
     in_specs = (
         P(("grp", "ep"), None),
@@ -91,4 +538,9 @@
         P("tp", None),
     )
     out_specs = P(("grp", "ep"), "tp")
-    return jax.shard_map(shards, mesh=mesh, in_specs=in_specs, out_specs=out_specs, check_vma=False)
+    def body(*args):
+        fits = mesh.shape["tp"] == 1 and mesh.shape["ep"] % 4 == 0 and args[4].shape[0] == 1
+        small = args[0].shape[0] * mesh.shape["ep"] <= args[4].shape[1]
+        return (fused_shards if fits and small else shards)(*args)
+
+    return jax.shard_map(body, mesh=mesh, in_specs=in_specs, out_specs=out_specs, check_vma=False)

time: 190 us -> 78.5 us (0.41)
  the two profiles are of different devices: /device:TPU:11 before, /device:TPU:0 now
where the time goes in v2:
time: 78.5 us; the launch traced here: 78.3 us
  Pallas kernels  73.9 us (94%)
  local copies, waits for them, and re-layouts  4.43 us (6%)
    pallas_call x1, Pallas kernels, fused_shards(): pl.pallas_call(functools.partial(fused_kernel, nz, pieces), out_shape=jax...  73.9 us
    unnamed x3, local copies, waits for them, and re-layouts  4.43 us

profile of v2, /device:TPU:0, one launch (start us, length us, event | category | flops | bytes accessed | tf_op | source)
XLA Modules:
  0.0 78.3 jit_solution(1488673799572709747)
XLA Ops:
  0.0 1.4 %copy.11.routes = s32[64,6]{1,0:T(8,128)} copy(s32[64,6]{0,1:T(8,128)} %param.12) | data formatting | bytes 3072 | tf_op args[2]
  1.4 1.4 %copy.12.gates = f32[64,6]{1,0:T(8,128)} copy(f32[64,6]{0,1:T(8,128)} %param.13) | data formatting | bytes 3072 | tf_op args[3]
  2.8 73.9 %shard_map.100 = bf16[64,2048]{1,0:T(8,128)(2,1)} custom-call(bf16[64,2048]{1,0:T(8,128)(2,1)} %tokens.1, f32[1,2048]{1,0:T(1,128)} %bitcast.7, s32[64,6]{1,0:T(8,128)} %copy.11.routes, f32[64,6]{1,0:T(8,128)} %copy.12.gates, bf16[2048,512]{1,0:T(8,128)(2,1)} %bitcast.4, bf16[2048,512]{1,0:T(8,128)(2,1)} %bitcast.5, bf16[512,2048]{1,0:T(8,128)(2,1)} %bitcast.6, ...), custom_call_target="tpu_custom_call" | custom-call | tf_op jit(solution)/shard_map/pallas_call | solution.py:470
  76.6 1.7 %copy.14 = bf16[64,2048]{1,0:T(8,128)(2,1)} copy(bf16[64,2048]{1,0:T(8,128)(2,1)} %shard_map.100) | data formatting | bytes 524288

commit v3 on v2

--- a/solution.py
+++ b/solution.py
@@ -223,13 +223,13 @@
     scale = lax.rsqrt(jnp.mean(values * values, axis=1, keepdims=True) + 1e-06)
     normed = (values * scale * gain[...]).astype(jnp.bfloat16)
     width = ag.shape[2] - cols
-    lane = lax.broadcasted_iota(jnp.int32, (rows, width), 1)
-    expert = lane % experts
-    weight = jnp.zeros((rows, width), jnp.float32)
-    for k in range(routes.shape[1]):
-        weight += jnp.where(expert == routes[:, k : k + 1], gates[:, k : k + 1], 0.0)
+    spots = lax.broadcasted_iota(jnp.int32, (width, rows), 0)
+    expert = spots % experts
+    weight = jnp.zeros((width, rows), jnp.float32)
+    for k in range(routes.shape[0]):
+        weight += jnp.where(expert == routes[k : k + 1, :], gates[k : k + 1, :], 0.0)
     high = weight.astype(jnp.bfloat16).astype(jnp.float32)
-    tail = jnp.where(lane < experts, high, jnp.where(lane < 2 * experts, weight - high, 0.0))
+    tail = jnp.where(spots < experts, high, jnp.where(spots < 2 * experts, weight - high, 0.0)).T
     ag[z, :rows, :cols] = normed
     ag[z, :rows, cols:] = tail.astype(jnp.bfloat16)
 
@@ -245,14 +245,6 @@
                 ag_z(z, 0, p, way).start()
 
         ag_d(z, 0, p).start()
-
-    for load in loads[:3]:
-        load.wait()
-    mine = ag[z, :rows, :cols]
-    gate = jnp.dot(mine, sg[...], preferred_element_type=jnp.float32)
-    lift = jnp.dot(mine, su[...], preferred_element_type=jnp.float32)
-    hidden = (jax.nn.silu(gate) * lift).astype(jnp.bfloat16)
-    shared[...] = jnp.dot(hidden, sd[...], preferred_element_type=jnp.float32)
 
     for p in sorted(count, key=lambda p: not pieces[p][2]):
         ag_x(z, p).wait_recv()
@@ -263,9 +255,6 @@
                 @pl.when(has(way))
                 def _():
                     ag_z(z, 1, p, way).start()
-
-    for load in loads[3:]:
-        load.wait()
 
     def at_distance(d, body):
         for way, layer, inside in ((0, z - d, z - d >= 0), (1, z + d, z + d < nz)):
@@ -372,6 +361,19 @@
     @pl.loop(0, nz)
     def _(k):
         at_distance(k + 1, forward)
+
+        @pl.when(k == 0)
+        def _():
+            for load in loads[:3]:
+                load.wait()
+            mine = ag[z, :rows, :cols]
+            gate = jnp.dot(mine, sg[...], preferred_element_type=jnp.float32)
+            lift = jnp.dot(mine, su[...], preferred_element_type=jnp.float32)
+            hidden = (jax.nn.silu(gate) * lift).astype(jnp.bfloat16)
+            shared[...] = jnp.dot(hidden, sd[...], preferred_element_type=jnp.float32)
+            for load in loads[3:]:
+                load.wait()
+
         experts_on(pick(order, k))
         at_distance(k + 1, relay)
 
@@ -508,8 +510,8 @@
     )(
         tokens,
         norm_gain[None, :],
-        routes,
-        gates,
+        routes.T,
+        gates.T,
         expert_gate[0],
         expert_up[0],
         expert_down[0],
@@ -521,7 +523,7 @@
 
 def make_pieces(rows):
     unit = rows // 4
-    return [(0, 2 * unit, False), (2 * unit, unit, False), (3 * unit, unit, True)]
+    return [(i * unit, unit, i == 3) for i in range(4)]
 
 
 def solution(mesh):

time: 78.5 us -> 74.4 us (0.948)
  local copies, waits for them, and re-layouts: 4.43 us -> 1.67 us
  Pallas kernels: 73.9 us -> 72.6 us
    unnamed x3 -> x1, local copies, waits for them, and re-layouts: 4.43 us -> 1.67 us
    pallas_call x1, Pallas kernels: 73.9 us -> 72.6 us  [fused_shards(): pl.pallas_call(functools.partial(fused_kernel, nz, pieces), out_shape=jax...]
where the time goes in v3:
time: 74.4 us; the launch traced here: 74.3 us
  Pallas kernels  72.6 us (98%)
  local copies, waits for them, and re-layouts  1.67 us (2%)
    pallas_call x1, Pallas kernels, fused_shards(): pl.pallas_call(functools.partial(fused_kernel, nz, pieces), out_shape=jax...  72.6 us
    unnamed x1, local copies, waits for them, and re-layouts  1.67 us

profile of v3, /device:TPU:0, one launch (start us, length us, event | category | flops | bytes accessed | tf_op | source)
XLA Modules:
  0.0 74.3 jit_solution(16225057169130746745)
XLA Ops:
  0.0 72.6 %shard_map.100 = bf16[64,2048]{1,0:T(8,128)(2,1)} custom-call(bf16[64,2048]{1,0:T(8,128)(2,1)} %tokens.1, f32[1,2048]{1,0:T(1,128)} %bitcast.9, s32[6,64]{1,0:T(8,128)} %bitcast.10, f32[6,64]{1,0:T(8,128)} %bitcast.11, bf16[2048,512]{1,0:T(8,128)(2,1)} %bitcast.6, bf16[2048,512]{1,0:T(8,128)(2,1)} %bitcast.7, bf16[512,2048]{1,0:T(8,128)(2,1)} %bitcast.8, ...), custom_call_target="tpu_custom_call" | custom-call | tf_op jit(solution)/shard_map/pallas_call | solution.py:472
  72.6 1.7 %copy.12 = bf16[64,2048]{1,0:T(8,128)(2,1)} copy(bf16[64,2048]{1,0:T(8,128)(2,1)} %shard_map.100) | data formatting | bytes 524288
